TPU v7x, 32 devices: a whole 2x2x4 slice. The times are simulated.
32 devices in a mesh: grp: 2 (over y), sp: 4 (over z), tp: 4 (over x, core).
Axes of the slice: x: 2, y: 2, z: 4, core: 2. Of those that a mesh axis runs over, the one named last changes fastest.
Arguments:
- query_rows: bfloat16 [1024, 1024], P(('grp', 'sp'), 'tp'), parts along dimension 0, may hold values from -6 to 6
- key_rows: bfloat16 [1024, 1024], P(('grp', 'sp'), 'tp'), parts along dimension 0, may hold values from -6 to 6
- value_rows: bfloat16 [1024, 1024], P(('grp', 'sp'), 'tp'), parts along dimension 0, may hold values from -6 to 6
- gate_rows: bfloat16 [1024, 1024], P(('grp', 'sp'), 'tp'), parts along dimension 0, may hold values from -6 to 6
- log_decay: float32 [2, 8, 1024], P(None, 'tp', ('grp', 'sp')), parts along dimension 2, may hold values from -2 to 0, as said below
- head_gain: float32 [2, 1024], P(None, 'tp'), may hold values from 0.1 to 1.9
- out_weight: bfloat16 [1024, 2048], P('tp'), may hold values from -0.1875 to 0.1875
- residual: bfloat16 [1024, 2048], P(('grp', 'sp')), parts along dimension 0, may hold values from -6 to 6
- norm_gain: bfloat16 [2048], replicated, may hold values from 0.099609375 to 1.8984375
- gate_weight: bfloat16 [2048, 5632], P('sp', 'tp'), may hold values from -0.125 to 0.125
- up_weight: bfloat16 [2048, 5632], P('sp', 'tp'), may hold values from -0.125 to 0.125
- down_weight: bfloat16 [2048, 5632], P('sp', 'tp'), may hold values from -0.078125 to 0.078125
- gate_taps: bfloat16 [3, 5632], P(None, 'tp'), may hold values from -3.5 to 3.5
- up_taps: bfloat16 [3, 5632], P(None, 'tp'), may hold values from -3.5 to 3.5
Outputs:
- block_out: bfloat16 [1024, 2048], P(('grp', 'sp', 'tp')), parts along dimension 0
There are 2 independent parts, one for each index of `grp`. A program takes and returns all parts, laid end to end along the dimension named above; an argument that names none is the same for every part. Nothing has to cross between parts.
Inputs may be any that keep to these rules, and one draw needn't show every extreme that they name: `log_decay`: every entry is negative.
All inputs are finite; a program needn't handle non-finite values.
Results may differ from a plain program's by a relative error of at most 0.017.
Values may be sent and summed in bfloat16 or wider, within the bound.
A program may use at most 64 MiB of HBM per device.

v0:
```python
import math

import jax
import jax.numpy as jnp
from jax import lax
from jax.sharding import PartitionSpec as P

HEAD = 128


FULL_PRECISION = lax.Precision.HIGHEST
GROUP_EPS = 1e-05
NORM_EPS = 1e-06


def prefix(value, axis, join, neutral, backward):
    count, mine = (lax.axis_size(axis), lax.axis_index(axis))
    pieces = jax.tree.map(lambda part: lax.all_gather(part, axis), value)
    if backward:
        pieces = jax.tree.map(lambda part: part[::-1], pieces)
        mine = count - 1 - mine
    running = jax.tree.map(
        lambda part, zero: jnp.full_like(part, 0) + jnp.asarray(zero, part.dtype), value, neutral
    )

    def lap(position, running):
        longer = join(running, jax.tree.map(lambda part: part[position], pieces))
        return jax.tree.map(lambda new, old: jnp.where(position < mine, new, old), longer, running)

    return lax.fori_loop(0, count - 1, lap, running)


def padded_2(shard, sides, width):
    for axis, dim in sides:
        size, length = (lax.axis_size(axis), shard.shape[dim])
        up = [(i, (i + 1) % size) for i in range(size - 1)]
        down = [(j, i) for i, j in up]
        last = lax.slice_in_dim(shard, length - width, length, axis=dim)
        initial = lax.slice_in_dim(shard, 0, width, axis=dim)
        before = lax.ppermute(last, axis, up)
        after = lax.ppermute(initial, axis, down)
        shard = jnp.concatenate([before, shard, after], axis=dim)
    return shard


def state_combine(earlier, later):
    return (earlier[0] * later[0], earlier[1] * later[0][:, None, None] + later[1])


def group_norm(values):
    length, head_count, head_width = values.shape
    centre = values - jnp.mean(values, axis=2, keepdims=True)
    spread = jnp.mean(centre * centre, axis=2, keepdims=True)
    return (centre * lax.rsqrt(spread + GROUP_EPS)).reshape(length, head_count * head_width)


def rms_scale(middle, gain):
    values = middle.astype(jnp.float32)
    multiplier = lax.rsqrt(jnp.mean(values * values, axis=1, keepdims=True) + NORM_EPS)
    return (values * multiplier * gain.astype(jnp.float32)).astype(jnp.bfloat16)


def local_retention(query_all, key_all, value_all, log_rates):
    length, head_count, head_width = query_all.shape
    block_len = math.gcd(length, 512)
    block_count = length // block_len
    cumul = jnp.cumsum(log_rates, axis=1).T
    query_block = query_all.reshape(block_count, block_len, head_count, head_width)
    key_block = key_all.reshape(block_count, block_len, head_count, head_width)
    value_block = value_all.reshape(block_count, block_len, head_count, head_width)
    cumul_block = cumul.reshape(block_count, block_len, head_count)
    before = jnp.concatenate(
        [jnp.zeros((1, head_count), jnp.float32), cumul_block[:-1, -1]], axis=0
    )
    local_cumul = cumul_block - before[:, None, :]
    gap_logs = local_cumul[:, :, None, :] - local_cumul[:, None, :, :]
    lower_mask = (jnp.arange(block_len)[:, None] >= jnp.arange(block_len)[None, :])[
        None, :, :, None
    ]
    decay_mask = jnp.where(lower_mask, jnp.exp(jnp.minimum(gap_logs, 0.0)), 0.0)
    scores = (
        jnp.einsum("bthd,bshd->btsh", query_block, key_block, precision=FULL_PRECISION) * decay_mask
    )
    inner_part = jnp.einsum("btsh,bshe->bthe", scores, value_block, precision=FULL_PRECISION)
    to_end = jnp.exp(local_cumul[:, -1:, :] - local_cumul)
    block_states = jnp.einsum(
        "bshd,bshe->bhde", key_block * to_end[..., None], value_block, precision=FULL_PRECISION
    )
    block_decay = jnp.exp(local_cumul[:, -1, :])

    def carry_step(carry_state, inputs):
        return (carry_state * inputs[0][:, None, None] + inputs[1], carry_state)

    zero_state = jnp.zeros((head_count, head_width, head_width), jnp.float32)
    end_state, entering = lax.scan(carry_step, zero_state, (block_decay, block_states))
    carried = jnp.einsum(
        "bthd,bhde->bthe",
        query_block * jnp.exp(local_cumul)[..., None],
        entering,
        precision=FULL_PRECISION,
    )
    output = (inner_part + carried).reshape(length, head_count, head_width)
    return (output, end_state, cumul, jnp.exp(cumul[-1]))


def with_incoming(output, query_all, cumul, incoming):
    return output + jnp.einsum(
        "thd,hde->the", query_all * jnp.exp(cumul)[:, :, None], incoming, precision=FULL_PRECISION
    )


def shards(
    query_rows,
    key_rows,
    value_rows,
    gate_rows,
    log_decay,
    head_gain,
    out_weight,
    residual,
    norm_gain,
    gate_weight,
    up_weight,
    down_weight,
    gate_taps,
    up_taps,
):
    pair_local = jnp.concatenate([gate_weight, up_weight], axis=1)
    row_count = query_rows.shape[0]
    head_count = query_rows.shape[1] // HEAD
    key_scale = HEAD ** (-0.5)
    query_all = query_rows.astype(jnp.float32).reshape(row_count, head_count, HEAD)
    key_all = key_rows.astype(jnp.float32).reshape(row_count, head_count, HEAD) * key_scale
    value_all = value_rows.astype(jnp.float32).reshape(row_count, head_count, HEAD)
    identity = (
        jnp.ones((head_count,), jnp.float32),
        jnp.zeros((head_count, HEAD, HEAD), jnp.float32),
    )
    ahead_local, ahead_state, ahead_cumul, ahead_decay = local_retention(
        query_all, key_all, value_all, log_decay[0]
    )
    query_back = query_all[::-1]
    behind_local, behind_state, behind_cumul, behind_decay = local_retention(
        query_back, key_all[::-1], value_all[::-1], log_decay[1][:, ::-1]
    )
    ahead_in = prefix((ahead_decay, ahead_state), "sp", state_combine, identity, False)[1]
    behind_in = prefix((behind_decay, behind_state), "sp", state_combine, identity, True)[1]
    ahead_out = with_incoming(ahead_local, query_all, ahead_cumul, ahead_in)
    behind_out = with_incoming(behind_local, query_back, behind_cumul, behind_in)[::-1]
    combined = group_norm(ahead_out) * head_gain[0] + group_norm(behind_out) * head_gain[1]
    mixed_heads = (jax.nn.silu(gate_rows.astype(jnp.float32)) * combined).astype(jnp.bfloat16)
    gathered = (
        lax.all_gather(pair_local, "sp", axis=0, tiled=True),
        lax.all_gather(down_weight, "sp", axis=0, tiled=True),
    )
    pair_full, down_full = gathered
    share_rows = row_count // lax.axis_size("tp")
    own_start = lax.axis_index("tp") * share_rows
    picked = mixed_heads
    attended = lax.psum_scatter(
        jnp.dot(picked, out_weight, preferred_element_type=jnp.float32).astype(jnp.bfloat16),
        "tp",
        scatter_dimension=0,
        tiled=True,
    ).astype(jnp.float32)
    residual_own = lax.dynamic_slice_in_dim(residual, own_start, share_rows, 0)
    middle_own = lax.optimization_barrier(
        (residual_own.astype(jnp.float32) + attended).astype(jnp.bfloat16)
    )
    normed = rms_scale(middle_own, norm_gain)
    pre_both = jnp.dot(
        lax.all_gather(normed, "tp", axis=0, tiled=True),
        pair_full,
        preferred_element_type=jnp.float32,
    ).astype(jnp.bfloat16)
    padded = padded_2(pre_both, (("sp", 0),), 1)
    half_width = gate_taps.shape[1]
    tap_table = jnp.concatenate([gate_taps, up_taps], axis=1).astype(jnp.float32)
    conv_out = (
        tap_table[0] * padded[:-2].astype(jnp.float32)
        + tap_table[1] * padded[1:-1].astype(jnp.float32)
        + tap_table[2] * padded[2:].astype(jnp.float32)
    )
    hidden = (jax.nn.silu(conv_out[:, :half_width]) * conv_out[:, half_width:]).astype(jnp.bfloat16)
    picked = hidden
    ff_out = lax.psum_scatter(
        lax.dot_general(
            picked, down_full, (((1,), (1,)), ((), ())), preferred_element_type=jnp.float32
        ).astype(jnp.bfloat16),
        "tp",
        scatter_dimension=0,
        tiled=True,
    ).astype(jnp.float32)
    return (middle_own.astype(jnp.float32) + ff_out).astype(jnp.bfloat16)


def solution(mesh):
    in_specs = (
        P(("grp", "sp"), "tp"),
        P(("grp", "sp"), "tp"),
        P(("grp", "sp"), "tp"),
        P(("grp", "sp"), "tp"),
        P(None, "tp", ("grp", "sp")),
        P(None, "tp"),
        P("tp", None),
        P(("grp", "sp"), None),
        P(),
        P("sp", "tp"),
        P("sp", "tp"),
        P("sp", "tp"),
        P(None, "tp"),
        P(None, "tp"),
    )
    out_specs = P(("grp", "sp", "tp"), None)
    return jax.shard_map(shards, mesh=mesh, in_specs=in_specs, out_specs=out_specs, check_vma=False)
```

profile of v0, /device:TPU:0, one launch (start us, length us, event | category | flops | bytes accessed | tf_op | source)
XLA Modules:
  0.0 416.1 jit_solution(4977097718532471524)
XLA Ops:
  7.4 0.8 slice_bitcast_fusion.1
  8.2 0.3 reduce_window_sum.17
  8.5 0.2 slice_reduce_fusion.1
  8.9 0.3 reduce_window_sum.18
  9.2 0.2 slice_reduce_fusion
  9.4 1.0 copy.89
  10.4 0.2 reverse.3
  10.6 0.9 bitcast_convert_fusion
  11.5 1.0 convolution_add_fusion
  12.5 17.5 %all-gather = f32[8,128,128]{2,1,0:T(8,128)S(1)} all-gather(f32[2,128,128]{2,1,0:T(8,128)S(1)} %convolution_add_fusion), channel_id=2, replica_groups=mesh['grp'=2,'sp'=4,'tp'=4] {'sp'}, dimensions={0}, use_global_device_ids=true | all-gather | bytes 655360 | tf_op jit(solution)/shard_map/all_gather | solution.py:18
  30.0 0.2 exponential_reduce_fusion.1
  30.2 11.7 %all-gather.2 = f32[4,1,2]{2,1,0:T(1,128)S(1)} all-gather(f32[1,1,2]{2,1,0:T(1,128)S(1)} %bitcast.179), channel_id=1, replica_groups=mesh['grp'=2,'sp'=4,'tp'=4] {'sp'}, dimensions={0}, use_global_device_ids=true | all-gather | bytes 40 | tf_op jit(solution)/shard_map/all_gather | solution.py:18
  41.9 0.4 while.18
  42.3 0.5 fusion.33
  42.7 0.4 convolution_bitcast_fusion.3
  43.2 0.3 fusion.9
  43.5 0.3 fusion.62
  43.9 0.3 convolution_add_fusion.1
  44.2 15.1 %all-gather.1 = f32[8,128,128]{2,1,0:T(8,128)S(1)} all-gather(f32[2,128,128]{2,1,0:T(8,128)S(1)} %convolution_add_fusion.1), channel_id=3, replica_groups=mesh['grp'=2,'sp'=4,'tp'=4] {'sp'}, dimensions={0}, use_global_device_ids=true | all-gather | bytes 655360 | tf_op jit(solution)/shard_map/all_gather | solution.py:18
  59.4 0.2 exponential_reduce_fusion
  59.6 8.0 %all-gather.3 = f32[4,1,2]{2,1,0:T(1,128)S(1)} all-gather(f32[1,1,2]{2,1,0:T(1,128)S(1)} %bitcast.180), channel_id=1, replica_groups=mesh['grp'=2,'sp'=4,'tp'=4] {'sp'}, dimensions={0}, use_global_device_ids=true | all-gather | bytes 40 | tf_op jit(solution)/shard_map/all_gather | solution.py:18
  67.9 0.4 while.19
  68.3 0.4 fusion.11
  68.7 0.3 fusion.30
  69.0 0.3 convolution_bitcast_fusion
  69.4 0.4 fusion.7
  69.8 0.1 reduce_sum.47
  70.0 0.2 multiply_reduce_fusion
  70.2 0.1 subtract_multiply_fusion
  70.5 0.1 copy.58
  70.6 0.1 fusion.28
  70.7 1.1 convolution_convert_fusion.1
  72.0 3.1 pad_maximum_fusion
  75.2 0.5 all-gather.9.cloned.1.call-update
  75.8 17.1 %reduce-scatter.3.cloned.1.call-done = bf16[32,2048]{1,0:T(8,128)(2,1)} async-done(((bf16[128,2048]{1,0:T(8,128)(2,1)}), bf16[32,2048]{1,0:T(8,128)(2,1)}) %reduce-scatter.3.cloned.1.call-update) | async-done | bytes 131088 | tf_op jit(solution)/shard_map/reduce_scatter | solution.py:160
  92.9 1.0 add_convert_fusion
  93.9 0.1 fusion.15
  94.2 6.6 %all_gather.29 = bf16[128,2048]{1,0:T(8,128)(2,1)S(1)} all-gather(bf16[32,2048]{1,0:T(8,128)(2,1)S(1)} %fusion.17), channel_id=1, replica_groups=mesh['grp'=2,'sp'=4,'tp'=4] {'tp'}, dimensions={0}, use_global_device_ids=true | all-gather | bytes 655360 | tf_op jit(solution)/shard_map/all_gather | solution.py:172
  100.8 174.5 %all-gather.7.cloned.1.call-done = bf16[2048,2816]{1,0:T(8,128)(2,1)} async-done(((bf16[512,2816]{1,0:T(8,128)(2,1)}), bf16[2048,2816]{1,0:T(8,128)(2,1)}) %all-gather.7.cloned.1.call-update) | async-done | bytes 11534352 | tf_op jit(solution)/shard_map/all_gather | solution.py:153
  275.3 5.9 %convolution_convert_fusion = bf16[128,2816]{1,0:T(8,128)(2,1)S(1)} fusion(bf16[128,2048]{1,0:T(8,128)(2,1)S(1)} %all_gather.29, bf16[2048,2816]{1,0:T(8,128)(2,1)} %all-gather.7.cloned.1.call-done), kind=kOutput, calls=%fused_computation.6 | convolution fusion | flops 1476755456 | bytes 12779520 | tf_op jit(solution)/shard_map/dot_general | solution.py:171
  281.3 1.3 collective-permute-start
  282.6 1.3 collective-permute-start.1
  284.1 4.6 %collective-permute-done.1 = bf16[1,2816]{1,0:T(2,128)(2,1)S(1)} collective-permute-done((bf16[1,2816]{1,0:T(2,128)(2,1)S(1)}, bf16[1,2816]{1,0:T(2,128)(2,1)S(1)}, u32[]{:S(2)}, u32[]{:S(2)}) %collective-permute-start.1) | collective-permute-done | bytes 5664 | tf_op jit(solution)/shard_map/ppermute | solution.py:41
  288.7 0.5 multiply_add_fusion
  289.2 92.5 %all-gather.9.cloned.1.call-done = bf16[2048,1408]{1,0:T(8,128)(2,1)} async-done(((bf16[512,1408]{1,0:T(8,128)(2,1)}), bf16[2048,1408]{1,0:T(8,128)(2,1)}) %all-gather.9.cloned.1.call-update) | async-done | bytes 5767184 | tf_op jit(solution)/shard_map/all_gather | solution.py:154
  381.7 5.4 %convolution_convert_fusion.2 = bf16[128,2048]{1,0:T(8,128)(2,1)} fusion(bf16[2048,1408]{1,0:T(8,128)(2,1)} %all-gather.9.cloned.1.call-done, f32[128,2816]{1,0:T(8,128)S(1)} %multiply_add_fusion), kind=kOutput, calls=%fused_computation.9 | convolution fusion | flops 739540992 | bytes 7733248 | tf_op jit(solution)/shard_map/dot_general | solution.py:187
  387.1 20.0 %reduce-scatter.5.cloned.1.call-done = bf16[32,2048]{1,0:T(8,128)(2,1)} async-done(((bf16[128,2048]{1,0:T(8,128)(2,1)}), bf16[32,2048]{1,0:T(8,128)(2,1)}) %reduce-scatter.5.cloned.1.call-update) | async-done | bytes 131088 | tf_op jit(solution)/shard_map/reduce_scatter | solution.py:186
  407.1 1.6 fusion.18
  (67 shorter events, 2.1 us)
Async XLA Ops:
  7.4 63.4 %copy-start = (bf16[256,2048]{1,0:T(8,128)(2,1)S(1)}, bf16[256,2048]{1,0:T(8,128)(2,1)}, u32[]{:S(2)}) copy-start(bf16[256,2048]{1,0:T(8,128)(2,1)} %param.24) | copy-start | bytes 3145732
  7.4 85.6 %reduce-scatter.3.cloned.1.call-start = ((), (), s32[]{:S(2)}) async-start(), calls=%async_computation.2 | async-start | bytes 655360 | tf_op jit(solution)/shard_map/reduce_scatter | solution.py:160
  12.5 29.7 %copy-start.2 = (bf16[128,256]{1,0:T(8,128)(2,1)S(1)}, bf16[128,256]{1,0:T(8,128)(2,1)}, u32[]{:S(2)}) copy-start(bf16[128,256]{1,0:T(8,128)(2,1)} %param.18) | copy-start | bytes 196612
  41.9 1.6 copy-start.3
  68.3 2.1 copy-start.8
  68.3 2.1 copy-start.4
  70.3 1.6 copy-start.1
  71.9 203.4 %all-gather.7.cloned.1.call-start = ((), (), s32[]{:S(2)}) async-start(), calls=%async_computation.3 | async-start | bytes 14417920 | tf_op jit(solution)/shard_map/all_gather | solution.py:153
  75.1 0.7 copy-start.7
  75.1 306.6 %all-gather.9.cloned.1.call-start = ((), (), s32[]{:S(2)}) async-start(), calls=%async_computation.4 | async-start | bytes 7208960 | tf_op jit(solution)/shard_map/all_gather | solution.py:154
  75.7 331.4 %reduce-scatter.5.cloned.1.call-start = ((), (), s32[]{:S(2)}) async-start(), calls=%async_computation.5 | async-start | bytes 655360 | tf_op jit(solution)/shard_map/reduce_scatter | solution.py:186
  100.8 183.1 %copy-start.5 = (bf16[3,1408]{1,0:T(4,128)(2,1)S(1)}, bf16[3,1408]{1,0:T(4,128)(2,1)}, u32[]{:S(2)}) copy-start(bf16[3,1408]{1,0:T(4,128)(2,1)} %param.31) | copy-start | bytes 25348
  100.8 183.1 %copy-start.6 = (bf16[3,1408]{1,0:T(4,128)(2,1)S(1)}, bf16[3,1408]{1,0:T(4,128)(2,1)}, u32[]{:S(2)}) copy-start(bf16[3,1408]{1,0:T(4,128)(2,1)} %param.30) | copy-start | bytes 25348
  281.3 2.7 collective-permute-start
  282.6 6.0 %collective-permute-start.1 = (bf16[1,2816]{1,0:T(2,128)(2,1)S(1)}, bf16[1,2816]{1,0:T(2,128)(2,1)S(1)}, u32[]{:S(2)}, u32[]{:S(2)}) collective-permute-start(bf16[1,2816]{1,0:T(2,128)(2,1)S(1)} %get-tuple-element.315), channel_id=1, source_target_pairs={{4,0},{8,4},{12,8},{5,1},{9,5},{13,9},{6,2},{10,6},{14,10},{7,3},{... | collective-permute-start | bytes 16904 | tf_op jit(solution)/shard_map/ppermute | solution.py:41
Sparse Core Ops, SparseCore 0:
  72.0 20.8 reduce-scatter.2
  387.2 19.8 reduce-scatter.4
Sparse Core Ops, SparseCore 1:
  75.2 200.1 all-gather.6
  276.8 104.8 all-gather.8
where the time goes:
time: 417 us; the launch traced here: 416 us
  waiting for transfers between devices  309 us (74%)
  blocking collectives  58.9 us (14%)
  matrix products  16.7 us (4%)
  between operations  15.2 us (4%)
  other arithmetic  9.4 us (2%)
    all_gather x1, waiting for transfers between devices, shards(): lax.all_gather(pair_local, 'sp', axis=0, tiled=True)  175 us
    all_gather x1, waiting for transfers between devices, shards(): lax.all_gather(down_weight, 'sp', axis=0, tiled=True)  92.5 us
    all_gather x4, blocking collectives, prefix(): pieces = jax.tree.map(lambda part: lax.all_gather(part, axis), value)  52.3 us
    reduce_scatter x1, waiting for transfers between devices, shards(): lax.psum_scatter(lax.dot_general(picked, down_full, (((1,), (1,)), ((), (...  20 us
    reduce_scatter x1, waiting for transfers between devices, shards(): lax.psum_scatter(jnp.dot(picked, out_weight, preferred_element_type=jnp.f...  17.1 us
  transfers between devices with their start and end apart: 6, of which 5 were waited for; matrix products, arithmetic and copies ran while one was open for 3% of the time, Pallas kernels for 0%

commit v1 on v0

--- a/solution.py
+++ b/solution.py
@@ -1,11 +1,15 @@
+import functools
 import math
 
 import jax
 import jax.numpy as jnp
 from jax import lax
+from jax.experimental import pallas as pl
+from jax.experimental.pallas import tpu as pltpu
 from jax.sharding import PartitionSpec as P
 
 HEAD = 128
+PIECES = 2
 
 
 FULL_PRECISION = lax.Precision.HIGHEST
@@ -194,6 +198,467 @@
     return (middle_own.astype(jnp.float32) + ff_out).astype(jnp.bfloat16)
 
 
+def block_kernel(
+    spans,
+    shares,
+    pieces,
+    query,
+    key,
+    value,
+    gate,
+    rates,
+    gains,
+    residual,
+    norm_gain,
+    gate_taps,
+    up_taps,
+    out_hbm,
+    gate_hbm,
+    up_hbm,
+    down_hbm,
+    result,
+    keys,
+    values,
+    rate_all,
+    out_w,
+    pair_w,
+    down_w,
+    att_send,
+    att_recv,
+    middle_ref,
+    norm_send,
+    norm_all,
+    part_send,
+    part_own,
+    part_recv,
+    rim_send,
+    rim_recv,
+    hidden_all,
+    tp_send,
+    tp_recv,
+    row_send,
+    row_recv,
+    local_sem,
+    kv_sem,
+    att_sem,
+    norm_sem,
+    fan_sem,
+    part_sem,
+    rim_sem,
+    hid_sem,
+    tp_sem,
+    row_sem,
+):
+    me, lane = lax.axis_index("sp"), lax.axis_index("tp")
+    rows, width = query.shape
+    heads = width // HEAD
+    share = rows // shares
+    model = residual.shape[1]
+    part_cols = model // spans
+    f32, bf16 = jnp.float32, jnp.bfloat16
+    sends = []
+
+    def send(src, dst, sems, sp, tp):
+        copy = pltpu.make_async_remote_copy(
+            src_ref=src,
+            dst_ref=dst,
+            send_sem=sems.at[0],
+            recv_sem=sems.at[1],
+            device_id={"sp": sp, "tp": tp},
+            device_id_type=pl.DeviceIdType.MESH,
+        )
+        copy.start()
+        sends.append(copy)
+        return copy
+
+    def span_at(step):
+        return lax.rem(me + step, spans)
+
+    def share_at(step):
+        return lax.rem(lane + step, shares)
+
+    def span_rows(index):
+        return pl.ds(pl.multiple_of(index * rows, rows), rows)
+
+    loads = [
+        pltpu.make_async_copy(src, dst, local_sem.at[i])
+        for i, (src, dst) in enumerate(
+            (
+                (key, keys.at[span_rows(me)]),
+                (value, values.at[span_rows(me)]),
+                (rates, rate_all.at[me]),
+                (out_hbm, out_w),
+                (gate_hbm, pair_w.at[0]),
+                (up_hbm, pair_w.at[1]),
+                (down_hbm, down_w),
+            )
+        )
+    ]
+    for load in loads:
+        load.start()
+    barrier = pltpu.get_barrier_semaphore()
+    for a in range(spans):
+        for b in range(shares):
+            if a or b:
+                pl.semaphore_signal(
+                    barrier,
+                    inc=1,
+                    device_id={"sp": span_at(a), "tp": share_at(b)},
+                    device_id_type=pl.DeviceIdType.MESH,
+                )
+    pl.semaphore_wait(barrier, spans * shares - 1)
+
+    arrivals = []
+    for d in range(1, spans):
+        to = span_at(d)
+        arrivals += [
+            send(rates, rate_all.at[me], kv_sem.at[d, 0], to, lane),
+            send(key, keys.at[span_rows(me)], kv_sem.at[d, 1], to, lane),
+            send(value, values.at[span_rows(me)], kv_sem.at[d, 2], to, lane),
+        ]
+    for load in loads[:3]:
+        load.wait()
+    for copy in arrivals:
+        copy.wait_recv()
+
+    low = lax.broadcasted_iota(jnp.int32, (rows, rows), 0)
+    high = lax.broadcasted_iota(jnp.int32, (rows, rows), 1)
+    upto = (low <= high).astype(f32)
+    since = (low >= high).astype(f32)
+    lines = rates.shape[0]
+    offset = jnp.zeros((lines, 1), f32)
+    offset_own = jnp.zeros((lines, 1), f32)
+    cumuls = []
+    for j in range(spans):
+        offset_own = jnp.where(j == me, offset, offset_own)
+        inside = jnp.dot(rate_all[j], upto, precision=FULL_PRECISION, preferred_element_type=f32)
+        cumuls.append(inside + offset)
+        offset = offset + inside[:, rows - 1 :]
+    cumul = jnp.concatenate(cumuls, axis=1)
+    every_rate = jnp.concatenate([rate_all[j] for j in range(spans)], axis=1)
+    own_rate = rates[...]
+    own_cumul = lax.dot_general(
+        since,
+        own_rate,
+        (((1,), (1,)), ((), ())),
+        precision=FULL_PRECISION,
+        preferred_element_type=f32,
+    )
+    own_before = lax.dot_general(
+        (low > high).astype(f32),
+        own_rate,
+        (((1,), (1,)), ((), ())),
+        precision=FULL_PRECISION,
+        preferred_element_type=f32,
+    )
+    total = spans * rows
+    mine_at = lax.broadcasted_iota(jnp.int32, (rows, total), 0) + me * rows
+    other_at = lax.broadcasted_iota(jnp.int32, (rows, total), 1)
+    mixed = []
+    for head in range(heads):
+        cols = slice(head * HEAD, (head + 1) * HEAD)
+        scores = lax.dot_general(
+            query[:, cols],
+            keys[:, cols],
+            (((1,), (1,)), ((), ())),
+            preferred_element_type=f32,
+        ) * (HEAD ** (-0.5))
+        back = heads + head
+        ahead_gap = (own_cumul[:, head : head + 1] + offset_own[head : head + 1]) - cumul[
+            head : head + 1
+        ]
+        behind_gap = (cumul[back : back + 1] - every_rate[back : back + 1]) - (
+            own_before[:, back : back + 1] + offset_own[back : back + 1]
+        )
+        sides = []
+        for gap, keep, row in (
+            (ahead_gap, mine_at >= other_at, 0),
+            (behind_gap, mine_at <= other_at, 1),
+        ):
+            weighted = jnp.where(keep, jnp.exp(jnp.minimum(gap, 0.0)), 0.0) * scores
+            top = weighted.astype(bf16)
+            rest = (weighted - top.astype(f32)).astype(bf16)
+            held = values[:, cols]
+            out = jnp.dot(top, held, preferred_element_type=f32) + jnp.dot(
+                rest, held, preferred_element_type=f32
+            )
+            centre = out - jnp.mean(out, axis=1, keepdims=True)
+            spread = jnp.mean(centre * centre, axis=1, keepdims=True)
+            sides.append(centre * lax.rsqrt(spread + GROUP_EPS) * gains[row : row + 1, cols])
+        level = gate[:, cols].astype(f32)
+        mixed.append(((level / (1.0 + jnp.exp(-level))) * (sides[0] + sides[1])).astype(bf16))
+    mixed = jnp.concatenate(mixed, axis=1)
+
+    loads[3].wait()
+    step_cols = math.gcd(model, 512)
+    for at in range(0, model, step_cols):
+        att_send[:, at : at + step_cols] = jnp.dot(
+            mixed, out_w[:, at : at + step_cols], preferred_element_type=f32
+        ).astype(bf16)
+
+    def share_rows(index):
+        return pl.ds(pl.multiple_of(index * share, share), share)
+
+    arrivals = [
+        send(
+            att_send.at[share_rows(share_at(d))],
+            att_recv.at[d],
+            att_sem.at[d],
+            me,
+            share_at(d),
+        )
+        for d in range(1, shares)
+    ]
+    attended = att_send[share_rows(lane), :].astype(f32)
+    for d, copy in enumerate(arrivals, 1):
+        copy.wait_recv()
+        attended = attended + att_recv[d].astype(f32)
+    middle = (residual[share_rows(lane), :].astype(f32) + attended).astype(bf16)
+    middle_ref[...] = middle
+    middle = middle.astype(f32)
+    factor = lax.rsqrt(jnp.mean(middle * middle, axis=1, keepdims=True) + NORM_EPS)
+    normed = (middle * factor * norm_gain[...].astype(f32)).astype(bf16)
+    for j in range(spans):
+        norm_send[j] = normed[:, j * part_cols : (j + 1) * part_cols]
+
+    def token_rows(span, tp):
+        return pl.ds(pl.multiple_of(span * rows + tp * share, share), share)
+
+    arrivals = [
+        send(
+            norm_send.at[span_at(d)],
+            norm_all.at[token_rows(me, lane)],
+            norm_sem.at[d],
+            span_at(d),
+            lane,
+        )
+        for d in range(1, spans)
+    ]
+    norm_all[token_rows(me, lane), :] = norm_send[me]
+    fans = {}
+    for d in (0, *range(1, spans)):
+        source = lax.rem(me + spans - d, spans)
+        if d:
+            arrivals[d - 1].wait_recv()
+        block = norm_send.at[me] if d == 0 else norm_all.at[token_rows(source, lane)]
+        for b in range(1, shares):
+            fans[d, b] = send(
+                block, norm_all.at[token_rows(source, lane)], fan_sem.at[d, b], me, share_at(b)
+            )
+    for copy in fans.values():
+        copy.wait_recv()
+
+    loads[4].wait()
+    loads[5].wait()
+    far_first = sorted(range(1, spans), key=lambda d: -min(d, spans - d))
+    parts = {}
+    for c, (start, size) in enumerate(pieces):
+        cols = slice(start, start + size)
+        for d in far_first + [0]:
+            block = norm_all[span_rows(span_at(d)), :]
+            for g in range(2):
+                product = jnp.dot(block, pair_w[g, :, cols], preferred_element_type=f32)
+                if d == 0:
+                    part_own[g, :, cols] = product
+                else:
+                    part_send[d, g, :, cols] = product.astype(bf16)
+            if d:
+                for g in range(2):
+                    parts[c, d, g] = send(
+                        part_send.at[d, g, :, pl.ds(start, size)],
+                        part_recv.at[d, g, :, pl.ds(start, size)],
+                        part_sem.at[c, d, g],
+                        span_at(d),
+                        lane,
+                    )
+
+    row_at = lax.broadcasted_iota(jnp.int32, (rows, 1), 0)
+    hidden_copies = {}
+    for c, (start, size) in enumerate(pieces):
+        cols = slice(start, start + size)
+        for d in range(1, spans):
+            for g in range(2):
+                parts[c, d, g].wait_recv()
+        for g in range(2):
+            summed = part_own[g, :, cols]
+            for d in range(1, spans):
+                summed = summed + part_recv[d, g, :, cols].astype(f32)
+            summed = summed.astype(bf16).astype(f32)
+            part_own[g, :, cols] = summed
+            rim_send[c, 0, g : g + 1, :size] = summed[rows - 1 :]
+            rim_send[c, 1, g : g + 1, :size] = summed[:1]
+        rims = [
+            send(
+                rim_send.at[c, way, :, pl.ds(0, size)],
+                rim_recv.at[c, way, :, pl.ds(0, size)],
+                rim_sem.at[c, way],
+                span_at(1 if way == 0 else spans - 1),
+                lane,
+            )
+            for way in range(2)
+        ]
+        for rim in rims:
+            rim.wait_recv()
+        convs = []
+        for g, taps in enumerate((gate_taps, up_taps)):
+            here = part_own[g, :, cols]
+            above = jnp.where(me > 0, rim_recv[c, 0, g : g + 1, :size], 0.0)
+            below = jnp.where(me < spans - 1, rim_recv[c, 1, g : g + 1, :size], 0.0)
+            earlier = jnp.where(row_at == 0, above, pltpu.roll(here, 1, 0))
+            later = jnp.where(row_at == rows - 1, below, pltpu.roll(here, rows - 1, 0))
+            weight = taps[:, cols].astype(f32)
+            convs.append(weight[0:1] * earlier + weight[1:2] * here + weight[2:3] * later)
+        hidden_all[span_rows(me), cols] = (
+            (convs[0] / (1.0 + jnp.exp(-convs[0]))) * convs[1]
+        ).astype(bf16)
+        for d in far_first:
+            block = hidden_all.at[span_rows(me), pl.ds(start, size)]
+            hidden_copies[c, d] = send(block, block, hid_sem.at[c, d], span_at(d), lane)
+
+    loads[6].wait()
+    near_first = [0] + far_first[::-1]
+    fans = {}
+    for d in near_first:
+        source = lax.rem(me + spans - d, spans)
+        if d:
+            for c in range(len(pieces)):
+                hidden_copies[c, d].wait_recv()
+        tp_send[d] = lax.dot_general(
+            hidden_all[span_rows(source), :],
+            down_w[...],
+            (((1,), (1,)), ((), ())),
+            preferred_element_type=f32,
+        ).astype(bf16)
+        for b in range(1, shares):
+            fans[d, b] = send(
+                tp_send.at[d, share_rows(share_at(b))],
+                tp_recv.at[d, b],
+                tp_sem.at[d, b],
+                me,
+                share_at(b),
+            )
+    arrivals = []
+    for d in near_first:
+        source = lax.rem(me + spans - d, spans)
+        summed = tp_send[d, share_rows(lane), :].astype(f32)
+        for b in range(1, shares):
+            fans[d, b].wait_recv()
+            summed = summed + tp_recv[d, b].astype(f32)
+        row_send[d] = summed.astype(bf16)
+        if d:
+            arrivals.append(send(row_send.at[d], row_recv.at[me], row_sem.at[d], source, lane))
+        else:
+            row_recv[me] = row_send[0]
+    for copy in arrivals:
+        copy.wait_recv()
+    for j in range(spans):
+        cols = slice(j * part_cols, (j + 1) * part_cols)
+        result[:, cols] = (middle_ref[:, cols].astype(f32) + row_recv[j].astype(f32)).astype(bf16)
+    for copy in sends:
+        copy.wait_send()
+
+
+def fused_block(
+    query_rows,
+    key_rows,
+    value_rows,
+    gate_rows,
+    log_decay,
+    head_gain,
+    out_weight,
+    residual,
+    norm_gain,
+    gate_weight,
+    up_weight,
+    down_weight,
+    gate_taps,
+    up_taps,
+):
+    spans, shares = (lax.axis_size("sp"), lax.axis_size("tp"))
+    rows, width = query_rows.shape
+    model = residual.shape[1]
+    units = gate_weight.shape[1]
+    part_cols, share = (model // spans, rows // shares)
+    total = spans * rows
+    lanes = units // 128
+    count = min(PIECES, lanes)
+    pieces, at = [], 0
+    for c in range(count):
+        size = (lanes // count + (c < lanes % count)) * 128
+        pieces.append((at, size))
+        at += size
+    widest = pieces[0][1]
+    lines = log_decay.shape[0] * log_decay.shape[1]
+    rates = log_decay.reshape(lines, rows)
+    f32, bf16 = jnp.float32, jnp.bfloat16
+    vmem = pl.BlockSpec(memory_space=pltpu.VMEM)
+    far = pl.BlockSpec(memory_space=pl.ANY)
+    dma = pltpu.SemaphoreType.DMA
+    return pl.pallas_call(
+        functools.partial(block_kernel, spans, shares, tuple(pieces)),
+        out_shape=jax.ShapeDtypeStruct((share, model), bf16),
+        in_specs=[vmem] * 10 + [far] * 4,
+        out_specs=vmem,
+        scratch_shapes=[
+            pltpu.VMEM((total, width), bf16),
+            pltpu.VMEM((total, width), bf16),
+            pltpu.VMEM((spans, lines, rows), f32),
+            pltpu.VMEM(out_weight.shape, bf16),
+            pltpu.VMEM((2, *gate_weight.shape), bf16),
+            pltpu.VMEM(down_weight.shape, bf16),
+            pltpu.VMEM((rows, model), bf16),
+            pltpu.VMEM((shares, share, model), bf16),
+            pltpu.VMEM((share, model), bf16),
+            pltpu.VMEM((spans, share, part_cols), bf16),
+            pltpu.VMEM((total, part_cols), bf16),
+            pltpu.VMEM((spans, 2, rows, units), bf16),
+            pltpu.VMEM((2, rows, units), f32),
+            pltpu.VMEM((spans, 2, rows, units), bf16),
+            pltpu.VMEM((count, 2, 2, widest), f32),
+            pltpu.VMEM((count, 2, 2, widest), f32),
+            pltpu.VMEM((total, units), bf16),
+            pltpu.VMEM((spans, rows, part_cols), bf16),
+            pltpu.VMEM((spans, shares, share, part_cols), bf16),
+            pltpu.VMEM((spans, share, part_cols), bf16),
+            pltpu.VMEM((spans, share, part_cols), bf16),
+            dma((7,)),
+            dma((spans, 3, 2)),
+            dma((shares, 2)),
+            dma((spans, 2)),
+            dma((spans, shares, 2)),
+            dma((count, spans, 2, 2)),
+            dma((count, 2, 2)),
+            dma((count, spans, 2)),
+            dma((spans, shares, 2)),
+            dma((spans, 2)),
+        ],
+        compiler_params=pltpu.CompilerParams(collective_id=0, has_side_effects=True),
+    )(
+        query_rows,
+        key_rows,
+        value_rows,
+        gate_rows,
+        rates,
+        head_gain,
+        residual,
+        norm_gain.reshape(1, model),
+        gate_taps,
+        up_taps,
+        out_weight,
+        gate_weight,
+        up_weight,
+        down_weight,
+    )
+
+
+def either(*args):
+    span_tokens = args[0].shape[0] * lax.axis_size("sp")
+    model_width = args[7].shape[1]
+    if span_tokens < model_width:
+        return fused_block(*args)
+    return shards(*args)
+
+
 def solution(mesh):
     in_specs = (
         P(("grp", "sp"), "tp"),
@@ -212,4 +677,4 @@
         P(None, "tp"),
     )
     out_specs = P(("grp", "sp", "tp"), None)
-    return jax.shard_map(shards, mesh=mesh, in_specs=in_specs, out_specs=out_specs, check_vma=False)
+    return jax.shard_map(either, mesh=mesh, in_specs=in_specs, out_specs=out_specs, check_vma=False)

time: 417 us -> 150 us (0.36)
  waiting for transfers between devices: 309 us -> 0 us
  Pallas kernels: 0 us -> 147 us
  blocking collectives: 58.9 us -> 0 us
  matrix products: 16.7 us -> 0 us
  between operations: 15.2 us -> 0.01 us
  other arithmetic: 9.4 us -> 0 us
    all_gather x2 -> x0, waiting for transfers between devices: 267 us -> none  [the longest x1 175 us: shards(): lax.all_gather(pair_local, 'sp', axis=0, tiled=True)]
    pallas_call x0 -> x1, Pallas kernels: none -> 147 us  [fused_block(): pl.pallas_call(functools.partial(block_kernel, spans, shares, tuple(piece...]
    all_gather x5 -> x0, blocking collectives: 58.9 us -> none  [the longest x4 52.3 us: prefix(): pieces = jax.tree.map(lambda part: lax.all_gather(part, axis), value)]
    reduce_scatter x2 -> x0, waiting for transfers between devices: 37.1 us -> none  [the longest x1 20 us: shards(): lax.psum_scatter(lax.dot_general(picked, down_full, (((1,), (1,)), ((), (...]
    dot_general x13 -> x0, matrix products: 16.7 us -> none  [the longest x1 5.95 us: shards(): jnp.dot(lax.all_gather(normed, 'tp', axis=0, tiled=True), pair_full, pref...]
    ppermute x2 -> x0, waiting for transfers between devices: 4.61 us -> none  [the longest x1 4.61 us: padded_2(): after = lax.ppermute(initial, axis, down)]
  transfers between devices with their start and end apart: 6 -> 0, of which waited for: 5 -> 0; matrix products, arithmetic and copies ran while one was open for 3% -> 0% of each run, Pallas kernels for 0% -> 0%
where the time goes in v1:
time: 150 us
  Pallas kernels  147 us (98%)
  local copies, waits for them, and re-layouts  2.86 us (2%)
    pallas_call x1, Pallas kernels, fused_block(): pl.pallas_call(functools.partial(block_kernel, spans, shares, tuple(piece...  147 us

profile of v1, /device:TPU:0, one launch (start us, length us, event | category | flops | bytes accessed | tf_op | source)
XLA Modules:
  0.0 149.8 jit_solution(10146788863041883411)
XLA Ops:
  0.0 1.3 reshape.7.norm_gain
  1.3 146.9 %shard_map.136 = bf16[32,2048]{1,0:T(8,128)(2,1)} custom-call(bf16[128,256]{1,0:T(8,128)(2,1)} %query.1, bf16[128,256]{1,0:T(8,128)(2,1)} %key.1, bf16[128,256]{1,0:T(8,128)(2,1)} %value.1, bf16[128,256]{1,0:T(8,128)(2,1)} %gate.1, f32[4,128]{1,0:T(4,128)} %bitcast.1, f32[2,256]{1,0:T(2,128)} %gains.1, bf16[128,2048]{1,0:T(8,128)(2,1)} %residual.1, ...), custom_call_target="tpu_custom_call" | custom-call | tf_op jit(solution)/shard_map/pallas_call | solution.py:597
  148.2 1.6 %copy.16 = bf16[32,2048]{1,0:T(8,128)(2,1)} copy(bf16[32,2048]{1,0:T(8,128)(2,1)} %shard_map.136) | data formatting | bytes 262144

commit v2 on v1

--- a/solution.py
+++ b/solution.py
@@ -9,7 +9,11 @@
 from jax.sharding import PartitionSpec as P
 
 HEAD = 128
-PIECES = 2
+PIECES = 12
+EDGE = 16
+FLIGHT = 2
+HEADSTART = 2
+SKEW = 2
 
 
 FULL_PRECISION = lax.Precision.HIGHEST
@@ -231,8 +235,6 @@
     part_send,
     part_own,
     part_recv,
-    rim_send,
-    rim_recv,
     hidden_all,
     tp_send,
     tp_recv,
@@ -244,7 +246,6 @@
     norm_sem,
     fan_sem,
     part_sem,
-    rim_sem,
     hid_sem,
     tp_sem,
     row_sem,
@@ -450,79 +451,138 @@
 
     loads[4].wait()
     loads[5].wait()
-    far_first = sorted(range(1, spans), key=lambda d: -min(d, spans - d))
-    parts = {}
-    for c, (start, size) in enumerate(pieces):
+    last = spans - 1
+    half = spans * rows // 2
+    reach = half + EDGE
+    size = pieces[0][1]
+    origins, owners = (last, 0), (0, last)
+
+    def part_copy(way, c):
+        return pltpu.make_async_remote_copy(
+            src_ref=part_send.at[way, c],
+            dst_ref=part_recv.at[way, c],
+            send_sem=part_sem.at[way, c, 0],
+            recv_sem=part_sem.at[way, c, 1],
+            device_id={"sp": span_at(spans - 1 if way == 0 else 1), "tp": lane},
+            device_id_type=pl.DeviceIdType.MESH,
+        )
+
+    def hidden_copy(way, c):
+        block = hidden_all.at[pl.ds(way * half, half), pl.ds(pieces[c][0], size)]
+        return pltpu.make_async_remote_copy(
+            src_ref=block,
+            dst_ref=block,
+            send_sem=hid_sem.at[way, c, 0],
+            recv_sem=hid_sem.at[way, c, 1],
+            device_id={"sp": span_at(1 if way == 0 else spans - 1), "tp": lane},
+            device_id_type=pl.DeviceIdType.MESH,
+        )
+
+    def start_part(way, c):
+        @pl.when(me == origins[way])
+        def _():
+            if c >= FLIGHT:
+                part_copy(way, c - FLIGHT).wait_send()
+            part_copy(way, c).start()
+
+    def start_hidden(way, c):
+        @pl.when(me == owners[way])
+        def _():
+            if c >= FLIGHT:
+                hidden_copy(way, c - FLIGHT).wait_send()
+            hidden_copy(way, c).start()
+
+    for c, (start, _) in enumerate(pieces):
         cols = slice(start, start + size)
-        for d in far_first + [0]:
-            block = norm_all[span_rows(span_at(d)), :]
-            for g in range(2):
-                product = jnp.dot(block, pair_w[g, :, cols], preferred_element_type=f32)
-                if d == 0:
-                    part_own[g, :, cols] = product
-                else:
-                    part_send[d, g, :, cols] = product.astype(bf16)
-            if d:
+        for way in range(2):
+            at = way * (half - EDGE)
+            block = norm_all[at : at + reach, :]
+            products = [
+                jnp.dot(block, pair_w[g, :, cols], preferred_element_type=f32) for g in range(2)
+            ]
+
+            @pl.when(me == origins[way])
+            def _():
                 for g in range(2):
-                    parts[c, d, g] = send(
-                        part_send.at[d, g, :, pl.ds(start, size)],
-                        part_recv.at[d, g, :, pl.ds(start, size)],
-                        part_sem.at[c, d, g],
-                        span_at(d),
-                        lane,
-                    )
-
-    row_at = lax.broadcasted_iota(jnp.int32, (rows, 1), 0)
-    hidden_copies = {}
-    for c, (start, size) in enumerate(pieces):
-        cols = slice(start, start + size)
-        for d in range(1, spans):
-            for g in range(2):
-                parts[c, d, g].wait_recv()
-        for g in range(2):
-            summed = part_own[g, :, cols]
-            for d in range(1, spans):
-                summed = summed + part_recv[d, g, :, cols].astype(f32)
-            summed = summed.astype(bf16).astype(f32)
-            part_own[g, :, cols] = summed
-            rim_send[c, 0, g : g + 1, :size] = summed[rows - 1 :]
-            rim_send[c, 1, g : g + 1, :size] = summed[:1]
-        rims = [
-            send(
-                rim_send.at[c, way, :, pl.ds(0, size)],
-                rim_recv.at[c, way, :, pl.ds(0, size)],
-                rim_sem.at[c, way],
-                span_at(1 if way == 0 else spans - 1),
-                lane,
-            )
-            for way in range(2)
-        ]
-        for rim in rims:
-            rim.wait_recv()
-        convs = []
-        for g, taps in enumerate((gate_taps, up_taps)):
-            here = part_own[g, :, cols]
-            above = jnp.where(me > 0, rim_recv[c, 0, g : g + 1, :size], 0.0)
-            below = jnp.where(me < spans - 1, rim_recv[c, 1, g : g + 1, :size], 0.0)
-            earlier = jnp.where(row_at == 0, above, pltpu.roll(here, 1, 0))
-            later = jnp.where(row_at == rows - 1, below, pltpu.roll(here, rows - 1, 0))
-            weight = taps[:, cols].astype(f32)
-            convs.append(weight[0:1] * earlier + weight[1:2] * here + weight[2:3] * later)
-        hidden_all[span_rows(me), cols] = (
-            (convs[0] / (1.0 + jnp.exp(-convs[0]))) * convs[1]
-        ).astype(bf16)
-        for d in far_first:
-            block = hidden_all.at[span_rows(me), pl.ds(start, size)]
-            hidden_copies[c, d] = send(block, block, hid_sem.at[c, d], span_at(d), lane)
+                    part_send[way, c, g] = products[g].astype(bf16)
+
+            if c < HEADSTART:
+                start_part(way, c)
+
+            @pl.when(me != origins[way])
+            def _():
+                for g in range(2):
+                    part_own[way, c, g] = products[g]
+
+    row_at = lax.broadcasted_iota(jnp.int32, (reach, 1), 0)
+    issued = 0
+    hops = (last - me, me)
+    for turn in range(len(pieces) + SKEW * (last - 1)):
+        if turn + HEADSTART < len(pieces):
+            for way in range(2):
+                start_part(way, turn + HEADSTART)
+        for way in range(2):
+            for hop in range(1, last):
+                c = turn - SKEW * (hop - 1)
+                if 0 <= c < len(pieces):
+
+                    @pl.when(hops[way] == hop)
+                    def _():
+                        part_copy(way, c).wait_recv()
+                        for g in range(2):
+                            part_send[way, c, g] = (
+                                part_own[way, c, g] + part_recv[way, c, g].astype(f32)
+                            ).astype(bf16)
+                        part_copy(way, c).start()
+
+            c = turn - SKEW * (last - 1)
+            if c < 0:
+                continue
+            cols = slice(pieces[c][0], pieces[c][0] + size)
+
+            @pl.when(me == owners[way])
+            def _():
+                part_copy(way, c).wait_recv()
+                convs = []
+                for g, taps in enumerate((gate_taps, up_taps)):
+                    here = (part_own[way, c, g] + part_recv[way, c, g].astype(f32)).astype(bf16)
+                    here = here.astype(f32)
+                    earlier, later = pltpu.roll(here, 1, 0), pltpu.roll(here, reach - 1, 0)
+                    if way == 0:
+                        earlier = jnp.where(row_at == 0, 0.0, earlier)
+                    else:
+                        later = jnp.where(row_at == reach - 1, 0.0, later)
+                    weight = taps[:, cols].astype(f32)
+                    convs.append(weight[0:1] * earlier + weight[1:2] * here + weight[2:3] * later)
+                hidden = ((convs[0] / (1.0 + jnp.exp(-convs[0]))) * convs[1]).astype(bf16)
+                at = way * EDGE
+                hidden_all[way * half : (way + 1) * half, cols] = hidden[at : at + half]
+
+        ready = min(max(0, turn - SKEW * (last - 1) + 1), len(pieces))
+        if ready < len(pieces):
+            ready = min(ready, 2 * max(0, turn + 1 + HEADSTART - len(pieces)))
+        while issued < ready:
+            for way in range(2):
+                start_hidden(way, issued)
+            issued += 1
+
+    for turn in range(len(pieces) + SKEW * (last - 1)):
+        for way in range(2):
+            for hop in range(1, spans):
+                c = turn - SKEW * (hop - 1)
+                if 0 <= c < len(pieces):
+
+                    @pl.when(last - hops[way] == hop)
+                    def _():
+                        hidden_copy(way, c).wait_recv()
+                        if hop < last:
+                            hidden_copy(way, c).start()
 
     loads[6].wait()
-    near_first = [0] + far_first[::-1]
+    near_first = list(range(spans))
     fans = {}
     for d in near_first:
         source = lax.rem(me + spans - d, spans)
-        if d:
-            for c in range(len(pieces)):
-                hidden_copies[c, d].wait_recv()
         tp_send[d] = lax.dot_general(
             hidden_all[span_rows(source), :],
             down_w[...],
@@ -556,6 +616,19 @@
         result[:, cols] = (middle_ref[:, cols].astype(f32) + row_recv[j].astype(f32)).astype(bf16)
     for copy in sends:
         copy.wait_send()
+    for c in range(len(pieces)):
+        for way in range(2):
+
+            middle_span = (me != owners[way]) & (me != origins[way])
+            unwaited = c + FLIGHT >= len(pieces)
+
+            @pl.when(middle_span | ((me == origins[way]) & unwaited))
+            def _():
+                part_copy(way, c).wait_send()
+
+            @pl.when(middle_span | ((me == owners[way]) & unwaited))
+            def _():
+                hidden_copy(way, c).wait_send()
 
 
 def fused_block(
@@ -581,13 +654,10 @@
     part_cols, share = (model // spans, rows // shares)
     total = spans * rows
     lanes = units // 128
-    count = min(PIECES, lanes)
-    pieces, at = [], 0
-    for c in range(count):
-        size = (lanes // count + (c < lanes % count)) * 128
-        pieces.append((at, size))
-        at += size
-    widest = pieces[0][1]
+    count = max(n for n in range(1, PIECES + 1) if lanes % n == 0)
+    size = units // count
+    pieces = [(c * size, size) for c in range(count)]
+    reach = total // 2 + EDGE
     lines = log_decay.shape[0] * log_decay.shape[1]
     rates = log_decay.reshape(lines, rows)
     f32, bf16 = jnp.float32, jnp.bfloat16
@@ -611,11 +681,9 @@
             pltpu.VMEM((share, model), bf16),
             pltpu.VMEM((spans, share, part_cols), bf16),
             pltpu.VMEM((total, part_cols), bf16),
-            pltpu.VMEM((spans, 2, rows, units), bf16),
-            pltpu.VMEM((2, rows, units), f32),
-            pltpu.VMEM((spans, 2, rows, units), bf16),
-            pltpu.VMEM((count, 2, 2, widest), f32),
-            pltpu.VMEM((count, 2, 2, widest), f32),
+            pltpu.VMEM((2, count, 2, reach, size), bf16),
+            pltpu.VMEM((2, count, 2, reach, size), f32),
+            pltpu.VMEM((2, count, 2, reach, size), bf16),
             pltpu.VMEM((total, units), bf16),
             pltpu.VMEM((spans, rows, part_cols), bf16),
             pltpu.VMEM((spans, shares, share, part_cols), bf16),
@@ -626,9 +694,8 @@
             dma((shares, 2)),
             dma((spans, 2)),
             dma((spans, shares, 2)),
-            dma((count, spans, 2, 2)),
-            dma((count, 2, 2)),
-            dma((count, spans, 2)),
+            dma((2, count, 2)),
+            dma((2, count, 2)),
             dma((spans, shares, 2)),
             dma((spans, 2)),
         ],

time: 150 us -> 116 us (0.77)
  Pallas kernels: 147 us -> 113 us
    pallas_call x1, Pallas kernels: 147 us -> 113 us  [fused_block(): pl.pallas_call(functools.partial(block_kernel, spans, shares, tuple(piece...]
where the time goes in v2:
time: 116 us; the launch traced here: 115 us
  Pallas kernels  113 us (97%)
  local copies, waits for them, and re-layouts  2.86 us (2%)
    pallas_call x1, Pallas kernels, fused_block(): pl.pallas_call(functools.partial(block_kernel, spans, shares, tuple(piece...  113 us

profile of v2, /device:TPU:0, one launch (start us, length us, event | category | flops | bytes accessed | tf_op | source)
XLA Modules:
  0.0 115.5 jit_solution(1396773738279995385)
XLA Ops:
  0.0 1.3 %reshape.7.norm_gain = bf16[1,2048]{1,0:T(2,128)(2,1)} reshape(bf16[2048]{0:T(1024)(128)(2,1)} %param.22) | data formatting | bytes 8192 | tf_op jit(solution)/shard_map/reshape | solution.py:711
  1.3 112.6 %shard_map.136 = bf16[32,2048]{1,0:T(8,128)(2,1)} custom-call(bf16[128,256]{1,0:T(8,128)(2,1)} %query.1, bf16[128,256]{1,0:T(8,128)(2,1)} %key.1, bf16[128,256]{1,0:T(8,128)(2,1)} %value.1, bf16[128,256]{1,0:T(8,128)(2,1)} %gate.1, f32[4,128]{1,0:T(4,128)} %bitcast.1, f32[2,256]{1,0:T(2,128)} %gains.1, bf16[128,2048]{1,0:T(8,128)(2,1)} %residual.1, ...), custom_call_target="tpu_custom_call" | custom-call | tf_op jit(solution)/shard_map/pallas_call | solution.py:667
  113.9 1.6 %copy.16 = bf16[32,2048]{1,0:T(8,128)(2,1)} copy(bf16[32,2048]{1,0:T(8,128)(2,1)} %shard_map.136) | data formatting | bytes 262144

commit v3 on v2

--- a/solution.py
+++ b/solution.py
@@ -492,8 +492,8 @@
                 hidden_copy(way, c - FLIGHT).wait_send()
             hidden_copy(way, c).start()
 
-    for c, (start, _) in enumerate(pieces):
-        cols = slice(start, start + size)
+    def project(c):
+        cols = slice(pieces[c][0], pieces[c][0] + size)
         for way in range(2):
             at = way * (half - EDGE)
             block = norm_all[at : at + reach, :]
@@ -506,21 +506,22 @@
                 for g in range(2):
                     part_send[way, c, g] = products[g].astype(bf16)
 
-            if c < HEADSTART:
-                start_part(way, c)
+            start_part(way, c)
 
             @pl.when(me != origins[way])
             def _():
                 for g in range(2):
                     part_own[way, c, g] = products[g]
+
+    for c in range(min(HEADSTART, len(pieces))):
+        project(c)
 
     row_at = lax.broadcasted_iota(jnp.int32, (reach, 1), 0)
     issued = 0
     hops = (last - me, me)
     for turn in range(len(pieces) + SKEW * (last - 1)):
         if turn + HEADSTART < len(pieces):
-            for way in range(2):
-                start_part(way, turn + HEADSTART)
+            project(turn + HEADSTART)
         for way in range(2):
             for hop in range(1, last):
                 c = turn - SKEW * (hop - 1)

time: 116 us -> 115 us (level)
  no operation moved by 1% of the time
where the time goes in v3:
time: 115 us
  Pallas kernels  112 us (97%)
  local copies, waits for them, and re-layouts  2.86 us (2%)
    pallas_call x1, Pallas kernels, fused_block(): pl.pallas_call(functools.partial(block_kernel, spans, shares, tuple(piece...  112 us

profile of v3, /device:TPU:0, one launch (start us, length us, event | category | flops | bytes accessed | tf_op | source)
XLA Modules:
  0.0 114.6 jit_solution(15502885379068143933)
XLA Ops:
  0.0 1.3 %reshape.7.norm_gain = bf16[1,2048]{1,0:T(2,128)(2,1)} reshape(bf16[2048]{0:T(1024)(128)(2,1)} %param.22) | data formatting | bytes 8192 | tf_op jit(solution)/shard_map/reshape | solution.py:712
  1.3 111.7 %shard_map.136 = bf16[32,2048]{1,0:T(8,128)(2,1)} custom-call(bf16[128,256]{1,0:T(8,128)(2,1)} %query.1, bf16[128,256]{1,0:T(8,128)(2,1)} %key.1, bf16[128,256]{1,0:T(8,128)(2,1)} %value.1, bf16[128,256]{1,0:T(8,128)(2,1)} %gate.1, f32[4,128]{1,0:T(4,128)} %bitcast.1, f32[2,256]{1,0:T(2,128)} %gains.1, bf16[128,2048]{1,0:T(8,128)(2,1)} %residual.1, ...), custom_call_target="tpu_custom_call" | custom-call | tf_op jit(solution)/shard_map/pallas_call | solution.py:668
  113.0 1.6 %copy.16 = bf16[32,2048]{1,0:T(8,128)(2,1)} copy(bf16[32,2048]{1,0:T(8,128)(2,1)} %shard_map.136) | data formatting | bytes 262144
